TPU v7x, 32 devices: a whole 2x2x4 slice. The times are simulated.
32 devices in a mesh: grp: 2 (over y), sp: 4 (over z), tp: 4 (over x, core).
Axes of the slice: x: 2, y: 2, z: 4, core: 2. Of those that a mesh axis runs over, the one named last changes fastest.
Arguments:
- tokens: bfloat16 [3072, 2048], P(('grp', 'sp'), 'tp'), parts along dimension 0, may hold values from -15 to 15
- gate_weight: bfloat16 [2, 2048, 2048], P(None, 'sp', 'tp'), may hold values from -0.125 to 0.125
- inner_weight: bfloat16 [2, 2048, 2048], P(None, 'sp', 'tp'), may hold values from -0.125 to 0.125
- value_weight: bfloat16 [2, 2048, 2048], P(None, 'sp', 'tp'), may hold values from -0.125 to 0.125
- out_weight: bfloat16 [2, 2048, 2048], P(None, 'tp', 'sp'), may hold values from -0.125 to 0.125
- taps: bfloat16 [2, 3, 2048], P(None, None, 'tp'), may hold values from -3 to 3
- norm_gain: float32 [2, 2048], P(None, 'tp'), may hold values from 0.1 to 1.9
- norm_bias: float32 [2, 2048], P(None, 'tp'), may hold values from -1.5 to 1.5
Outputs:
- mixed: bfloat16 [3072, 2048], P(('grp', 'sp'), 'tp'), parts along dimension 0
There are 2 independent parts, one for each index of `grp`. A program takes and returns all parts, laid end to end along the dimension named above; an argument that names none is the same for every part. Nothing has to cross between parts.
All inputs are finite; a program needn't handle non-finite values.
Results may differ from a plain program's by a relative error of at most 0.03.
Values may be sent and summed in bfloat16 or wider, within the bound.
No kernel may reach another device: no remote copies, remote signals or barrier semaphores. Data moves between devices by JAX's collectives and lax.ppermute only.
A program may use at most 64 MiB of HBM per device.

v0:
```python
import jax
import jax.numpy as jnp
from jax import lax
from jax.sharding import PartitionSpec as P

LAYERS = 2


def extended(value, sides, width):
    for axis, dim in sides:
        peers, length = (lax.axis_size(axis), value.shape[dim])
        up = [(i, (i + 1) % peers) for i in range(peers - 1)]
        down = [(j, i) for i, j in up]
        last = lax.slice_in_dim(value, length - width, length, axis=dim)
        initial = lax.slice_in_dim(value, 0, width, axis=dim)
        before = lax.ppermute(last, axis, up)
        after = lax.ppermute(initial, axis, down)
        value = jnp.concatenate([before, value, after], axis=dim)
    return value


def shards(tokens, gate_weight, inner_weight, value_weight, out_weight, taps, norm_gain, norm_bias):
    x = tokens
    width = x.shape[1] * lax.axis_size("tp")
    full_gate, full_inner, full_value, full_out = (
        lax.all_gather(gate_weight, "sp", axis=1, tiled=True),
        lax.all_gather(inner_weight, "sp", axis=1, tiled=True),
        lax.all_gather(value_weight, "sp", axis=1, tiled=True),
        lax.all_gather(out_weight, "sp", axis=2, tiled=True),
    )
    for layer in range(LAYERS):
        whole = lax.all_gather(x, "tp", axis=1, tiled=True)
        outer = jnp.dot(whole, full_gate[layer], preferred_element_type=jnp.float32)
        inner = jnp.dot(whole, full_inner[layer], preferred_element_type=jnp.float32)
        values = jnp.dot(whole, full_value[layer], preferred_element_type=jnp.float32)
        outer = outer.astype(jnp.bfloat16)
        inner = inner.astype(jnp.bfloat16)
        values = values.astype(jnp.bfloat16)
        product = (inner.astype(jnp.float32) * values.astype(jnp.float32)).astype(jnp.bfloat16)
        padded = extended(product, (("sp", 0),), 1).astype(jnp.float32)
        kernel = taps[layer].astype(jnp.float32)
        conv = kernel[0] * padded[:-2] + kernel[1] * padded[1:-1] + kernel[2] * padded[2:]
        gated = (outer.astype(jnp.float32) * conv).astype(jnp.bfloat16)
        terms = jnp.dot(gated, full_out[layer], preferred_element_type=jnp.float32)
        branch = lax.psum_scatter(
            terms.astype(jnp.bfloat16), "tp", scatter_dimension=1, tiled=True
        ).astype(jnp.float32)
        total = 2.0**0.5 * x.astype(jnp.float32) + branch
        row_sum, row_square = lax.psum(
            (jnp.sum(total, axis=1), jnp.sum(total * total, axis=1)), "tp"
        )
        mean = (row_sum / width)[:, None]
        spread = (row_square / width)[:, None] - mean * mean
        x = (
            (total - mean) * lax.rsqrt(spread + 1e-05) * norm_gain[layer] + norm_bias[layer]
        ).astype(jnp.bfloat16)
    return x


def solution(mesh):
    in_specs = (
        P(("grp", "sp"), "tp"),
        P(None, "sp", "tp"),
        P(None, "sp", "tp"),
        P(None, "sp", "tp"),
        P(None, "tp", "sp"),
        P(None, None, "tp"),
        P(None, "tp"),
        P(None, "tp"),
    )
    out_specs = P(("grp", "sp"), "tp")
    return jax.shard_map(shards, mesh=mesh, in_specs=in_specs, out_specs=out_specs, check_vma=False)
```

profile of v0, /device:TPU:0, one launch (start us, length us, event | category | flops | bytes accessed | tf_op | source)
XLA Modules:
  0.0 479.8 jit_solution(8200364497382368189)
XLA Ops:
  6.5 0.0 all-gather.7.cloned.1.call-start
  6.5 0.7 all-gather.7.cloned.1.call-update
  7.3 0.0 copy-start.2
  7.3 0.0 all-gather.13.cloned.1.call-start
  7.3 0.7 all-gather.13.cloned.1.call-update
  8.0 0.0 all-gather.11.cloned.1.call-start
  8.1 0.7 all-gather.11.cloned.1.call-update
  8.8 0.0 all-gather.15.cloned.1.call-start
  8.8 0.5 all-gather.15.cloned.1.call-update
  9.3 0.0 all-gather.9.cloned.1.call-start
  9.4 0.5 all-gather.9.cloned.1.call-update
  9.9 0.0 reduce-scatter.3.cloned.1.call-start
  10.0 0.0 copy-done.2
  10.0 21.3 %all-gather.7.cloned.1.call-done = bf16[384,2048]{1,0:T(8,128)(2,1)} async-done(((bf16[384,512]{1,0:T(8,128)(2,1)}), bf16[384,2048]{1,0:T(8,128)(2,1)}) %all-gather.7.cloned.1.call-update) | async-done | bytes 1572880 | tf_op jit(solution)/shard_map/all_gather | solution.py:32
  31.3 0.0 copy-start.6
  31.3 82.3 %all-gather.13.cloned.1.call-done = bf16[2,2048,512]{2,1,0:T(8,128)(2,1)} async-done(((bf16[2,512,512]{2,1,0:T(8,128)(2,1)}), bf16[2,2048,512]{2,1,0:T(8,128)(2,1)}) %all-gather.13.cloned.1.call-update) | async-done | bytes 4194320 | tf_op jit(solution)/shard_map/all_gather | solution.py:28
  113.6 3.0 fusion.15
  116.7 77.8 %all-gather.11.cloned.1.call-done = bf16[2,2048,512]{2,1,0:T(8,128)(2,1)} async-done(((bf16[2,512,512]{2,1,0:T(8,128)(2,1)}), bf16[2,2048,512]{2,1,0:T(8,128)(2,1)}) %all-gather.11.cloned.1.call-update) | async-done | bytes 4194320 | tf_op jit(solution)/shard_map/all_gather | solution.py:27
  194.5 0.0 copy-done.6
  194.5 2.6 fusion.13
  197.0 1.3 collective-permute-start
  198.3 1.3 collective-permute-start.1
  199.7 0.0 collective-permute-done
  199.7 4.2 collective-permute-done.1
  203.9 0.1 maximum_convert_fusion
  204.0 71.1 %all-gather.15.cloned.1.call-done = bf16[2,512,2048]{2,1,0:T(8,128)(2,1)} async-done(((bf16[2,512,512]{2,1,0:T(8,128)(2,1)}), bf16[2,512,2048]{2,1,0:T(8,128)(2,1)}) %all-gather.15.cloned.1.call-update) | async-done | bytes 4194320 | tf_op jit(solution)/shard_map/all_gather | solution.py:29
  275.1 80.7 %all-gather.9.cloned.1.call-done = bf16[2,2048,512]{2,1,0:T(8,128)(2,1)} async-done(((bf16[2,512,512]{2,1,0:T(8,128)(2,1)}), bf16[2,2048,512]{2,1,0:T(8,128)(2,1)}) %all-gather.9.cloned.1.call-update) | async-done | bytes 4194320 | tf_op jit(solution)/shard_map/all_gather | solution.py:26
  355.8 0.0 copy-start.3
  355.8 0.0 copy-start.4
  355.8 0.0 copy-start.1
  355.8 5.4 %convolution_convert_fusion.1 = bf16[384,2048]{1,0:T(8,128)(2,1)} fusion(bf16[2,512,2048]{2,1,0:T(8,128)(2,1)} %all-gather.15.cloned.1.call-done, bf16[384,2048]{1,0:T(8,128)(2,1)S(1)} %copy-done.6, bf16[2,2048,512]{2,1,0:T(8,128)(2,1)} %all-gather.9.cloned.1.call-done, f32[386,512]{1,0:T(8,128)S(1)} %maximum_convert_fusion, f32[512]{0:T(512)S(1)} %bitcast.92, ...), kind=kOutput, calls=%fused_computation.1 | convolution fusion | flops 1613168640 | bytes 9705472 | tf_op jit(solution)/shard_map/dot_general | solution.py:44
  361.2 0.0 reduce-scatter.3.cloned.1.call-update
  361.2 0.0 all-gather.17.cloned.1.call-start
  361.3 0.0 copy-done.3
  361.3 0.0 copy-done.4
  361.3 26.6 %reduce-scatter.3.cloned.1.call-done = bf16[384,512]{1,0:T(8,128)(2,1)} async-done(((bf16[384,2048]{1,0:T(8,128)(2,1)}), bf16[384,512]{1,0:T(8,128)(2,1)}) %reduce-scatter.3.cloned.1.call-update) | async-done | bytes 393232 | tf_op jit(solution)/shard_map/reduce_scatter | solution.py:45
  387.9 0.0 copy-done.1
  387.9 1.3 fusion.34
  389.2 5.8 %all-reduce.1 = (f32[384]{0:T(512)S(1)}, f32[384]{0:T(512)S(1)}) all-reduce(f32[384]{0:T(512)S(1)} %get-tuple-element.8, f32[384]{0:T(512)S(1)} %get-tuple-element.7), channel_id=1, replica_groups=mesh['grp'=2,'sp'=4,'tp'=4] {'tp'}, use_global_device_ids=true, to_apply=%region_4.0 | all-reduce | flops 768 | bytes 6144 | tf_op jit(solution)/shard_map/psum | solution.py:49
  395.0 2.0 add_convert_fusion.1
  397.0 0.0 all-gather.17.cloned.1.call-update
  397.0 0.0 reduce-scatter.5.cloned.1.call-start
  397.0 20.3 %all-gather.17.cloned.1.call-done = bf16[384,2048]{1,0:T(8,128)(2,1)} async-done(((bf16[384,512]{1,0:T(8,128)(2,1)}), bf16[384,2048]{1,0:T(8,128)(2,1)}) %all-gather.17.cloned.1.call-update) | async-done | bytes 1572880 | tf_op jit(solution)/shard_map/all_gather | solution.py:32
  417.4 0.0 copy-start.5
  417.4 0.0 copy-start.7
  417.4 3.2 fusion.25
  420.6 0.1 copy-done.5
  420.7 0.5 copy-done.7
  421.2 1.0 fusion.23
  422.2 3.4 collective-permute-start.2
  425.5 1.3 collective-permute-start.3
  426.8 0.0 collective-permute-done.2
  426.9 4.2 collective-permute-done.3
  431.0 0.1 maximum_convert_fusion.1
  431.1 0.0 copy-start
  431.2 5.5 %convolution_convert_fusion = bf16[384,2048]{1,0:T(8,128)(2,1)} fusion(bf16[2,512,2048]{2,1,0:T(8,128)(2,1)} %all-gather.15.cloned.1.call-done, bf16[384,2048]{1,0:T(8,128)(2,1)S(1)} %copy-done.7, bf16[2,2048,512]{2,1,0:T(8,128)(2,1)} %all-gather.9.cloned.1.call-done, f32[386,512]{1,0:T(8,128)S(1)} %maximum_convert_fusion.1, f32[512]{0:T(512)S(1)} %bitcast.89, ...), kind=kOutput, calls=%fused_computation | convolution fusion | flops 1613168640 | bytes 9705472 | tf_op jit(solution)/shard_map/dot_general | solution.py:44
  436.6 0.0 reduce-scatter.5.cloned.1.call-update
  436.7 27.3 %reduce-scatter.5.cloned.1.call-done = bf16[384,512]{1,0:T(8,128)(2,1)} async-done(((bf16[384,2048]{1,0:T(8,128)(2,1)}), bf16[384,512]{1,0:T(8,128)(2,1)}) %reduce-scatter.5.cloned.1.call-update) | async-done | bytes 393232 | tf_op jit(solution)/shard_map/reduce_scatter | solution.py:45
  464.0 0.0 copy-done
  464.0 1.3 fusion.35
  465.2 5.8 %all-reduce = (f32[384]{0:T(512)S(1)}, f32[384]{0:T(512)S(1)}) all-reduce(f32[384]{0:T(512)S(1)} %get-tuple-element.6, f32[384]{0:T(512)S(1)} %get-tuple-element.5), channel_id=1, replica_groups=mesh['grp'=2,'sp'=4,'tp'=4] {'tp'}, use_global_device_ids=true, to_apply=%region_9.0 | all-reduce | flops 768 | bytes 6144 | tf_op jit(solution)/shard_map/psum | solution.py:49
  471.0 2.0 add_convert_fusion
  (8 shorter events, 0.1 us)
Async XLA Ops:
  6.5 24.7 %all-gather.7.cloned.1.call-start = ((), (), s32[]{:S(2)}) async-start(), calls=%async_computation.2 | async-start | bytes 1966080 | tf_op jit(solution)/shard_map/all_gather | solution.py:32
  7.3 2.7 copy-start.2
  7.3 106.4 %all-gather.13.cloned.1.call-start = ((), (), s32[]{:S(2)}) async-start(), calls=%async_computation.5 | async-start | bytes 5242880 | tf_op jit(solution)/shard_map/all_gather | solution.py:28
  8.0 186.4 %all-gather.11.cloned.1.call-start = ((), (), s32[]{:S(2)}) async-start(), calls=%async_computation.4 | async-start | bytes 5242880 | tf_op jit(solution)/shard_map/all_gather | solution.py:27
  8.8 266.4 %all-gather.15.cloned.1.call-start = ((), (), s32[]{:S(2)}) async-start(), calls=%async_computation.6 | async-start | bytes 5242880 | tf_op jit(solution)/shard_map/all_gather | solution.py:29
  9.3 346.5 %all-gather.9.cloned.1.call-start = ((), (), s32[]{:S(2)}) async-start(), calls=%async_computation.3 | async-start | bytes 5242880 | tf_op jit(solution)/shard_map/all_gather | solution.py:26
  9.9 378.0 %reduce-scatter.3.cloned.1.call-start = ((), (), s32[]{:S(2)}) async-start(), calls=%async_computation.7 | async-start | bytes 1966080 | tf_op jit(solution)/shard_map/reduce_scatter | solution.py:45
  31.3 163.2 %copy-start.6 = (bf16[384,2048]{1,0:T(8,128)(2,1)S(1)}, bf16[384,2048]{1,0:T(8,128)(2,1)}, u32[]{:S(2)}) copy-start(bf16[384,2048]{1,0:T(8,128)(2,1)} %all-gather.7.cloned.1.call-done) | copy-start | bytes 4718596
  197.0 2.6 collective-permute-start
  198.3 5.6 %collective-permute-start.1 = (bf16[1,512]{1,0:T(2,128)(2,1)S(1)}, bf16[1,512]{1,0:T(2,128)(2,1)S(1)}, u32[]{:S(2)}, u32[]{:S(2)}) collective-permute-start(bf16[1,512]{1,0:T(2,128)(2,1)S(1)} %get-tuple-element.16), channel_id=1, source_target_pairs={{4,0},{8,4},{12,8},{5,1},{9,5},{13,9},{6,2},{10,6},{14,10},{7,3},{... | collective-permute-start | bytes 3080 | tf_op jit(solution)/shard_map/ppermute | solution.py:17
  355.8 5.5 %copy-start.3 = (f32[2,512]{1,0:T(2,128)S(1)}, f32[2,512]{1,0:T(2,128)}, u32[]{:S(2)}) copy-start(f32[2,512]{1,0:T(2,128)} %param.14) | copy-start | bytes 12292
  355.8 5.5 %copy-start.4 = (f32[2,512]{1,0:T(2,128)S(1)}, f32[2,512]{1,0:T(2,128)}, u32[]{:S(2)}) copy-start(f32[2,512]{1,0:T(2,128)} %param.15) | copy-start | bytes 12292
  355.8 32.1 %copy-start.1 = (bf16[384,512]{1,0:T(8,128)(2,1)S(1)}, bf16[384,512]{1,0:T(8,128)(2,1)}, u32[]{:S(2)}) copy-start(bf16[384,512]{1,0:T(8,128)(2,1)} %param.8) | copy-start | bytes 1179652
  361.2 56.1 %all-gather.17.cloned.1.call-start = ((), (), s32[]{:S(2)}) async-start(), calls=%async_computation.8 | async-start | bytes 1966080 | tf_op jit(solution)/shard_map/all_gather | solution.py:32
  397.0 67.0 %reduce-scatter.5.cloned.1.call-start = ((), (), s32[]{:S(2)}) async-start(), calls=%async_computation.9 | async-start | bytes 1966080 | tf_op jit(solution)/shard_map/reduce_scatter | solution.py:45
  417.4 3.3 copy-start.5
  417.4 3.8 copy-start.7
  422.2 4.7 collective-permute-start.2
  425.5 5.5 %collective-permute-start.3 = (bf16[1,512]{1,0:T(2,128)(2,1)S(1)}, bf16[1,512]{1,0:T(2,128)(2,1)S(1)}, u32[]{:S(2)}, u32[]{:S(2)}) collective-permute-start(bf16[1,512]{1,0:T(2,128)(2,1)S(1)} %get-tuple-element.14), channel_id=1, source_target_pairs={{4,0},{8,4},{12,8},{5,1},{9,5},{13,9},{6,2},{10,6},{14,10},{7,3},{... | collective-permute-start | bytes 3080 | tf_op jit(solution)/shard_map/ppermute | solution.py:17
  431.1 32.8 %copy-start = (bf16[384,512]{1,0:T(8,128)(2,1)S(1)}, bf16[384,512]{1,0:T(8,128)(2,1)}, u32[]{:S(2)}) copy-start(bf16[384,512]{1,0:T(8,128)(2,1)} %add_convert_fusion.1) | copy-start | bytes 1179652
Sparse Core Ops, SparseCore 0:
  8.9 22.3 all-gather.6
  32.8 80.7 all-gather.12
  115.2 79.2 all-gather.10
  195.9 79.2 all-gather.14
  276.6 79.2 all-gather.8
  361.4 26.5 reduce-scatter.2
  397.1 20.2 all-gather.16
  436.8 27.1 reduce-scatter.4
where the time goes:
time: 480 us
  waiting for transfers between devices  419 us (87%)
  matrix products  20.6 us (4%)
  between operations  13.7 us (3%)
  blocking collectives  11.5 us (2%)
  starting transfers between devices  7.54 us (2%)
  other arithmetic  6.74 us (1%)
    all_gather x1, waiting for transfers between devices, shards(): lax.all_gather(value_weight, 'sp', axis=1, tiled=True)  82.3 us
    all_gather x1, waiting for transfers between devices, shards(): lax.all_gather(gate_weight, 'sp', axis=1, tiled=True)  80.7 us
    all_gather x1, waiting for transfers between devices, shards(): lax.all_gather(inner_weight, 'sp', axis=1, tiled=True)  77.8 us
    all_gather x1, waiting for transfers between devices, shards(): lax.all_gather(out_weight, 'sp', axis=2, tiled=True)  71.1 us
    reduce_scatter x2, waiting for transfers between devices, shards(): lax.psum_scatter(terms.astype(jnp.bfloat16), 'tp', scatter_dimension=1, t...  53.9 us
    all_gather x2, waiting for transfers between devices, shards(): whole = lax.all_gather(x, 'tp', axis=1, tiled=True)  41.6 us
    psum x2, blocking collectives, shards(): lax.psum((jnp.sum(total, axis=1), jnp.sum(total * total, axis=1)), 'tp')  11.5 us
    dot_general x2, matrix products, shards(): terms = jnp.dot(gated, full_out[layer], preferred_element_type=jnp.float32)  10.9 us
  transfers between devices with their start and end apart: 12, of which 10 were waited for; matrix products, arithmetic and copies ran while one was open for 1% of the time, Pallas kernels for 0%

commit v1 on v0

--- a/solution.py
+++ b/solution.py
@@ -29,7 +29,13 @@
         lax.all_gather(out_weight, "sp", axis=2, tiled=True),
     )
     for layer in range(LAYERS):
-        whole = lax.all_gather(x, "tp", axis=1, tiled=True)
+        count = lax.axis_size("tp")
+        moving, blocks = (x, [x])
+        for _ in range(count - 1):
+            moving = lax.ppermute(moving, "tp", [(i_2, (i_2 + 1) % count) for i_2 in range(count)])
+            blocks.insert(0, moving)
+        merged = jnp.concatenate(blocks, axis=1)
+        whole = jnp.roll(merged, (lax.axis_index("tp") + 1) * x.shape[1], axis=1)
         outer = jnp.dot(whole, full_gate[layer], preferred_element_type=jnp.float32)
         inner = jnp.dot(whole, full_inner[layer], preferred_element_type=jnp.float32)
         values = jnp.dot(whole, full_value[layer], preferred_element_type=jnp.float32)

time: 480 us -> 461 us (0.960)
  waiting for transfers between devices: 419 us -> 397 us
    ppermute x0 -> x6, waiting for transfers between devices: none -> 43.3 us  [shards(): lax.ppermute(moving, 'tp', [(i_2, (i_2 + 1) % count) for i_2 in range(cou...]
    all_gather x2 -> x0, waiting for transfers between devices: 41.6 us -> none  [shards(): whole = lax.all_gather(x, 'tp', axis=1, tiled=True)]
    all_gather x1, waiting for transfers between devices: 82.3 us -> 58.6 us  [shards(): lax.all_gather(value_weight, 'sp', axis=1, tiled=True)]
  transfers between devices with their start and end apart: 12 -> 16, of which waited for: 10 -> 14; matrix products, arithmetic and copies ran while one was open for 1% -> 2% of each run, Pallas kernels for 0% -> 0%
where the time goes in v1:
time: 461 us; the launch traced here: 460 us
  waiting for transfers between devices  397 us (86%)
  matrix products  17.8 us (4%)
  between operations  13.7 us (3%)
  blocking collectives  11.5 us (2%)
  other arithmetic  10.2 us (2%)
  starting transfers between devices  8.28 us (2%)
    all_gather x1, waiting for transfers between devices, shards(): lax.all_gather(gate_weight, 'sp', axis=1, tiled=True)  80.7 us
    all_gather x1, waiting for transfers between devices, shards(): lax.all_gather(inner_weight, 'sp', axis=1, tiled=True)  78.3 us
    all_gather x1, waiting for transfers between devices, shards(): lax.all_gather(out_weight, 'sp', axis=2, tiled=True)  71.3 us
    all_gather x1, waiting for transfers between devices, shards(): lax.all_gather(value_weight, 'sp', axis=1, tiled=True)  58.6 us
    reduce_scatter x2, waiting for transfers between devices, shards(): lax.psum_scatter(terms.astype(jnp.bfloat16), 'tp', scatter_dimension=1, t...  54.2 us
    ppermute x6, waiting for transfers between devices, shards(): lax.ppermute(moving, 'tp', [(i_2, (i_2 + 1) % count) for i_2 in range(cou...  43.3 us
    psum x2, blocking collectives, shards(): lax.psum((jnp.sum(total, axis=1), jnp.sum(total * total, axis=1)), 'tp')  11.5 us
    dot_general x2, matrix products, shards(): terms = jnp.dot(gated, full_out[layer], preferred_element_type=jnp.float32)  10.7 us
  transfers between devices with their start and end apart: 16, of which 14 were waited for; matrix products, arithmetic and copies ran while one was open for 2% of the time, Pallas kernels for 0%

profile of v1, /device:TPU:0, one launch (start us, length us, event | category | flops | bytes accessed | tf_op | source)
XLA Modules:
  0.0 460.2 jit_solution(4481613327264194451)
XLA Ops:
  6.5 0.0 copy-start
  6.5 0.0 copy-start.1
  6.5 0.0 all-gather.9.cloned.1.call-start
  6.5 0.7 all-gather.9.cloned.1.call-update
  7.3 0.0 all-gather.7.cloned.1.call-start
  7.3 0.7 all-gather.7.cloned.1.call-update
  8.0 0.0 all-gather.11.cloned.1.call-start
  8.1 0.7 all-gather.11.cloned.1.call-update
  8.7 0.0 all-gather.5.cloned.1.call-start
  8.8 0.5 all-gather.5.cloned.1.call-update
  9.3 0.0 reduce-scatter.3.cloned.1.call-start
  9.4 0.0 copy-done
  9.4 0.5 collective-permute-start
  9.9 7.4 %collective-permute-done = bf16[384,512]{1,0:T(8,128)(2,1)S(1)} collective-permute-done((bf16[384,512]{1,0:T(8,128)(2,1)S(1)}, bf16[384,512]{1,0:T(8,128)(2,1)S(1)}, u32[]{:S(2)}, u32[]{:S(2)}) %collective-permute-start) | collective-permute-done | bytes 393248 | tf_op jit(solution)/shard_map/ppermute | solution.py:35
  17.3 0.0 collective-permute-start.1
  17.3 7.2 %collective-permute-done.1 = bf16[384,512]{1,0:T(8,128)(2,1)S(1)} collective-permute-done((bf16[384,512]{1,0:T(8,128)(2,1)S(1)}, bf16[384,512]{1,0:T(8,128)(2,1)S(1)}, u32[]{:S(2)}, u32[]{:S(2)}) %collective-permute-start.1) | collective-permute-done | bytes 393248 | tf_op jit(solution)/shard_map/ppermute | solution.py:35
  24.5 0.0 collective-permute-start.2
  24.5 0.0 copy-done.1
  24.5 7.2 %collective-permute-done.2 = bf16[384,512]{1,0:T(8,128)(2,1)S(1)} collective-permute-done((bf16[384,512]{1,0:T(8,128)(2,1)S(1)}, bf16[384,512]{1,0:T(8,128)(2,1)S(1)}, u32[]{:S(2)}, u32[]{:S(2)}) %collective-permute-start.2) | collective-permute-done | bytes 393248 | tf_op jit(solution)/shard_map/ppermute | solution.py:35
  31.7 2.0 fusion.16
  33.8 58.6 %all-gather.9.cloned.1.call-done = bf16[2,2048,512]{2,1,0:T(8,128)(2,1)} async-done(((bf16[2,512,512]{2,1,0:T(8,128)(2,1)}), bf16[2,2048,512]{2,1,0:T(8,128)(2,1)}) %all-gather.9.cloned.1.call-update) | async-done | bytes 4194320 | tf_op jit(solution)/shard_map/all_gather | solution.py:28
  92.4 2.6 fusion.29
  95.0 78.3 %all-gather.7.cloned.1.call-done = bf16[2,2048,512]{2,1,0:T(8,128)(2,1)} async-done(((bf16[2,512,512]{2,1,0:T(8,128)(2,1)}), bf16[2,2048,512]{2,1,0:T(8,128)(2,1)}) %all-gather.7.cloned.1.call-update) | async-done | bytes 4194320 | tf_op jit(solution)/shard_map/all_gather | solution.py:27
  173.2 2.6 fusion.27
  175.8 1.3 collective-permute-start.3
  177.1 1.3 collective-permute-start.4
  178.4 0.0 collective-permute-done.3
  178.4 4.2 collective-permute-done.4
  182.7 0.1 maximum_convert_fusion
  182.8 71.3 %all-gather.11.cloned.1.call-done = bf16[2,512,2048]{2,1,0:T(8,128)(2,1)} async-done(((bf16[2,512,512]{2,1,0:T(8,128)(2,1)}), bf16[2,512,2048]{2,1,0:T(8,128)(2,1)}) %all-gather.11.cloned.1.call-update) | async-done | bytes 4194320 | tf_op jit(solution)/shard_map/all_gather | solution.py:29
  254.1 80.7 %all-gather.5.cloned.1.call-done = bf16[2,2048,512]{2,1,0:T(8,128)(2,1)} async-done(((bf16[2,512,512]{2,1,0:T(8,128)(2,1)}), bf16[2,2048,512]{2,1,0:T(8,128)(2,1)}) %all-gather.5.cloned.1.call-update) | async-done | bytes 4194320 | tf_op jit(solution)/shard_map/all_gather | solution.py:26
  334.7 0.0 copy-start.2
  334.8 5.4 %convolution_convert_fusion.1 = bf16[384,2048]{1,0:T(8,128)(2,1)} fusion(bf16[2,512,2048]{2,1,0:T(8,128)(2,1)} %all-gather.11.cloned.1.call-done, bf16[384,2048]{1,0:T(8,128)(2,1)S(1)} %fusion.16, bf16[2,2048,512]{2,1,0:T(8,128)(2,1)} %all-gather.5.cloned.1.call-done, f32[386,512]{1,0:T(8,128)S(1)} %maximum_convert_fusion, f32[512]{0:T(512)S(1)} %bitcast.92, ...), kind=kOutput, calls=%fused_computation.17 | convolution fusion | flops 1613168640 | bytes 9705472 | tf_op jit(solution)/shard_map/dot_general | solution.py:50
  340.1 0.0 reduce-scatter.3.cloned.1.call-update
  340.1 0.0 reduce-scatter.5.cloned.1.call-start
  340.2 0.0 copy-done.2
  340.2 0.0 copy-done.3
  340.2 26.5 %reduce-scatter.3.cloned.1.call-done = bf16[384,512]{1,0:T(8,128)(2,1)} async-done(((bf16[384,2048]{1,0:T(8,128)(2,1)}), bf16[384,512]{1,0:T(8,128)(2,1)}) %reduce-scatter.3.cloned.1.call-update) | async-done | bytes 393232 | tf_op jit(solution)/shard_map/reduce_scatter | solution.py:51
  366.8 1.3 fusion.48
  368.0 5.8 %all-reduce.1 = (f32[384]{0:T(512)S(1)}, f32[384]{0:T(512)S(1)}) all-reduce(f32[384]{0:T(512)S(1)} %get-tuple-element.9, f32[384]{0:T(512)S(1)} %get-tuple-element.8), channel_id=1, replica_groups=mesh['grp'=2,'sp'=4,'tp'=4] {'tp'}, use_global_device_ids=true, to_apply=%region_4.6 | all-reduce | flops 768 | bytes 6144 | tf_op jit(solution)/shard_map/psum | solution.py:55
  373.8 1.4 add_convert_fusion.1
  375.2 0.1 collective-permute-start.5
  375.2 7.2 %collective-permute-done.5 = bf16[384,512]{1,0:T(8,128)(2,1)S(1)} collective-permute-done((bf16[384,512]{1,0:T(8,128)(2,1)S(1)}, bf16[384,512]{1,0:T(8,128)(2,1)S(1)}, u32[]{:S(2)}, u32[]{:S(2)}) %collective-permute-start.5) | collective-permute-done | bytes 393248 | tf_op jit(solution)/shard_map/ppermute | solution.py:35
  382.4 0.0 collective-permute-start.6
  382.4 7.2 %collective-permute-done.6 = bf16[384,512]{1,0:T(8,128)(2,1)S(1)} collective-permute-done((bf16[384,512]{1,0:T(8,128)(2,1)S(1)}, bf16[384,512]{1,0:T(8,128)(2,1)S(1)}, u32[]{:S(2)}, u32[]{:S(2)}) %collective-permute-start.6) | collective-permute-done | bytes 393248 | tf_op jit(solution)/shard_map/ppermute | solution.py:35
  389.6 0.0 collective-permute-start.7
  389.6 7.2 %collective-permute-done.7 = bf16[384,512]{1,0:T(8,128)(2,1)S(1)} collective-permute-done((bf16[384,512]{1,0:T(8,128)(2,1)S(1)}, bf16[384,512]{1,0:T(8,128)(2,1)S(1)}, u32[]{:S(2)}, u32[]{:S(2)}) %collective-permute-start.7) | collective-permute-done | bytes 393248 | tf_op jit(solution)/shard_map/ppermute | solution.py:35
  396.8 2.0 fusion.9
  398.9 0.0 copy-done.4
  398.9 0.0 copy-start.5
  398.9 1.0 fusion.39
  399.9 1.2 copy-done.5
  401.1 1.0 fusion.37
  402.1 3.6 collective-permute-start.8
  405.7 1.3 collective-permute-start.9
  407.0 0.0 collective-permute-done.8
  407.0 4.2 collective-permute-done.9
  411.2 0.1 maximum_convert_fusion.1
  411.3 5.4 %convolution_convert_fusion = bf16[384,2048]{1,0:T(8,128)(2,1)} fusion(bf16[2,512,2048]{2,1,0:T(8,128)(2,1)} %all-gather.11.cloned.1.call-done, bf16[384,2048]{1,0:T(8,128)(2,1)S(1)} %fusion.9, bf16[2,2048,512]{2,1,0:T(8,128)(2,1)} %all-gather.5.cloned.1.call-done, f32[386,512]{1,0:T(8,128)S(1)} %maximum_convert_fusion.1, f32[512]{0:T(512)S(1)} %bitcast.89, ...), kind=kOutput, calls=%fused_computation.16 | convolution fusion | flops 1613168640 | bytes 9705472 | tf_op jit(solution)/shard_map/dot_general | solution.py:50
  416.7 0.0 reduce-scatter.5.cloned.1.call-update
  416.7 27.6 %reduce-scatter.5.cloned.1.call-done = bf16[384,512]{1,0:T(8,128)(2,1)} async-done(((bf16[384,2048]{1,0:T(8,128)(2,1)}), bf16[384,512]{1,0:T(8,128)(2,1)}) %reduce-scatter.5.cloned.1.call-update) | async-done | bytes 393232 | tf_op jit(solution)/shard_map/reduce_scatter | solution.py:51
  444.3 1.3 fusion.49
  445.6 5.8 %all-reduce = (f32[384]{0:T(512)S(1)}, f32[384]{0:T(512)S(1)}) all-reduce(f32[384]{0:T(512)S(1)} %get-tuple-element.7, f32[384]{0:T(512)S(1)} %get-tuple-element.6), channel_id=1, replica_groups=mesh['grp'=2,'sp'=4,'tp'=4] {'tp'}, use_global_device_ids=true, to_apply=%region_9.11 | all-reduce | flops 768 | bytes 6144 | tf_op jit(solution)/shard_map/psum | solution.py:55
  451.3 2.0 add_convert_fusion
  (10 shorter events, 0.1 us)
Async XLA Ops:
  6.5 2.8 copy-start
  6.5 18.0 %copy-start.1 = (bf16[2,3,512]{2,0,1:T(2,128)(2,1)S(1)}, bf16[2,3,512]{2,0,1:T(2,128)(2,1)}, u32[]{:S(2)}) copy-start(bf16[2,3,512]{2,0,1:T(2,128)(2,1)} %param.15) | copy-start | bytes 18436
  6.5 85.9 %all-gather.9.cloned.1.call-start = ((), (), s32[]{:S(2)}) async-start(), calls=%async_computation.4 | async-start | bytes 5242880 | tf_op jit(solution)/shard_map/all_gather | solution.py:28
  7.3 166.0 %all-gather.7.cloned.1.call-start = ((), (), s32[]{:S(2)}) async-start(), calls=%async_computation.3 | async-start | bytes 5242880 | tf_op jit(solution)/shard_map/all_gather | solution.py:27
  8.0 246.1 %all-gather.11.cloned.1.call-start = ((), (), s32[]{:S(2)}) async-start(), calls=%async_computation.5 | async-start | bytes 5242880 | tf_op jit(solution)/shard_map/all_gather | solution.py:29
  8.7 326.0 %all-gather.5.cloned.1.call-start = ((), (), s32[]{:S(2)}) async-start(), calls=%async_computation.2 | async-start | bytes 5242880 | tf_op jit(solution)/shard_map/all_gather | solution.py:26
  9.3 357.4 %reduce-scatter.3.cloned.1.call-start = ((), (), s32[]{:S(2)}) async-start(), calls=%async_computation.6 | async-start | bytes 1966080 | tf_op jit(solution)/shard_map/reduce_scatter | solution.py:51
  9.4 7.9 %collective-permute-start = (bf16[384,512]{1,0:T(8,128)(2,1)S(1)}, bf16[384,512]{1,0:T(8,128)(2,1)S(1)}, u32[]{:S(2)}, u32[]{:S(2)}) collective-permute-start(bf16[384,512]{1,0:T(8,128)(2,1)S(1)} %copy-done), channel_id=1, source_target_pairs={{0,1},{1,2},{2,3},{3,0},{4,5},{5,6},{6,7},{7,4},{8,9},{9,10},{10,1... | collective-permute-start | bytes 1179656 | tf_op jit(solution)/shard_map/ppermute | solution.py:35
  17.3 7.2 %collective-permute-start.1 = (bf16[384,512]{1,0:T(8,128)(2,1)S(1)}, bf16[384,512]{1,0:T(8,128)(2,1)S(1)}, u32[]{:S(2)}, u32[]{:S(2)}) collective-permute-start(bf16[384,512]{1,0:T(8,128)(2,1)S(1)} %collective-permute-done), channel_id=1, source_target_pairs={{0,1},{1,2},{2,3},{3,0},{4,5},{5,6},{6,7},{7,4},{8,9},{9,10},{10,1... | collective-permute-start | bytes 1179656 | tf_op jit(solution)/shard_map/ppermute | solution.py:35
  24.5 7.2 %collective-permute-start.2 = (bf16[384,512]{1,0:T(8,128)(2,1)S(1)}, bf16[384,512]{1,0:T(8,128)(2,1)S(1)}, u32[]{:S(2)}, u32[]{:S(2)}) collective-permute-start(bf16[384,512]{1,0:T(8,128)(2,1)S(1)} %collective-permute-done.1), channel_id=1, source_target_pairs={{0,1},{1,2},{2,3},{3,0},{4,5},{5,6},{6,7},{7,4},{8,9},{9,10},{10,1... | collective-permute-start | bytes 1179656 | tf_op jit(solution)/shard_map/ppermute | solution.py:35
  175.8 2.6 collective-permute-start.3
  177.1 5.6 %collective-permute-start.4 = (bf16[1,512]{1,0:T(2,128)(2,1)S(1)}, bf16[1,512]{1,0:T(2,128)(2,1)S(1)}, u32[]{:S(2)}, u32[]{:S(2)}) collective-permute-start(bf16[1,512]{1,0:T(2,128)(2,1)S(1)} %get-tuple-element.17), channel_id=1, source_target_pairs={{4,0},{8,4},{12,8},{5,1},{9,5},{13,9},{6,2},{10,6},{14,10},{7,3},{... | collective-permute-start | bytes 3080 | tf_op jit(solution)/shard_map/ppermute | solution.py:17
  334.7 5.4 %copy-start.2 = (f32[2,512]{1,0:T(2,128)S(1)}, f32[2,512]{1,0:T(2,128)}, u32[]{:S(2)}) copy-start(f32[2,512]{1,0:T(2,128)} %param.16) | copy-start | bytes 12292
  334.8 5.5 %copy-start.3 = (f32[2,512]{1,0:T(2,128)S(1)}, f32[2,512]{1,0:T(2,128)}, u32[]{:S(2)}) copy-start(f32[2,512]{1,0:T(2,128)} %param.17) | copy-start | bytes 12292
  340.1 104.2 %reduce-scatter.5.cloned.1.call-start = ((), (), s32[]{:S(2)}) async-start(), calls=%async_computation.7 | async-start | bytes 1966080 | tf_op jit(solution)/shard_map/reduce_scatter | solution.py:51
  373.8 25.1 %copy-start.4 = (bf16[2,2048,512]{2,1,0:T(8,128)(2,1)S(1)}, bf16[2,2048,512]{2,1,0:T(8,128)(2,1)}, u32[]{:S(2)}) copy-start(bf16[2,2048,512]{2,1,0:T(8,128)(2,1)} %all-gather.9.cloned.1.call-done) | copy-start | bytes 12582916
  375.2 7.3 %collective-permute-start.5 = (bf16[384,512]{1,0:T(8,128)(2,1)S(1)}, bf16[384,512]{1,0:T(8,128)(2,1)S(1)}, u32[]{:S(2)}, u32[]{:S(2)}) collective-permute-start(bf16[384,512]{1,0:T(8,128)(2,1)S(1)} %add_convert_fusion.1), channel_id=1, source_target_pairs={{0,1},{1,2},{2,3},{3,0},{4,5},{5,6},{6,7},{7,4},{8,9},{9,10},{10,1... | collective-permute-start | bytes 1179656 | tf_op jit(solution)/shard_map/ppermute | solution.py:35
  382.4 7.2 %collective-permute-start.6 = (bf16[384,512]{1,0:T(8,128)(2,1)S(1)}, bf16[384,512]{1,0:T(8,128)(2,1)S(1)}, u32[]{:S(2)}, u32[]{:S(2)}) collective-permute-start(bf16[384,512]{1,0:T(8,128)(2,1)S(1)} %collective-permute-done.5), channel_id=1, source_target_pairs={{0,1},{1,2},{2,3},{3,0},{4,5},{5,6},{6,7},{7,4},{8,9},{9,10},{10,1... | collective-permute-start | bytes 1179656 | tf_op jit(solution)/shard_map/ppermute | solution.py:35
  389.6 7.2 %collective-permute-start.7 = (bf16[384,512]{1,0:T(8,128)(2,1)S(1)}, bf16[384,512]{1,0:T(8,128)(2,1)S(1)}, u32[]{:S(2)}, u32[]{:S(2)}) collective-permute-start(bf16[384,512]{1,0:T(8,128)(2,1)S(1)} %collective-permute-done.6), channel_id=1, source_target_pairs={{0,1},{1,2},{2,3},{3,0},{4,5},{5,6},{6,7},{7,4},{8,9},{9,10},{10,1... | collective-permute-start | bytes 1179656 | tf_op jit(solution)/shard_map/ppermute | solution.py:35
  398.9 2.2 copy-start.5
  402.1 4.9 %collective-permute-start.8 = (bf16[1,512]{1,0:T(2,128)(2,1)S(1)}, bf16[1,512]{1,0:T(2,128)(2,1)S(1)}, u32[]{:S(2)}, u32[]{:S(2)}) collective-permute-start(bf16[1,512]{1,0:T(2,128)(2,1)S(1)} %get-tuple-element.14), channel_id=1, source_target_pairs={{0,4},{4,8},{8,12},{1,5},{5,9},{9,13},{2,6},{6,10},{10,14},{3,7},{... | collective-permute-start | bytes 3080 | tf_op jit(solution)/shard_map/ppermute | solution.py:16
  405.7 5.5 %collective-permute-start.9 = (bf16[1,512]{1,0:T(2,128)(2,1)S(1)}, bf16[1,512]{1,0:T(2,128)(2,1)S(1)}, u32[]{:S(2)}, u32[]{:S(2)}) collective-permute-start(bf16[1,512]{1,0:T(2,128)(2,1)S(1)} %get-tuple-element.15), channel_id=1, source_target_pairs={{4,0},{8,4},{12,8},{5,1},{9,5},{13,9},{6,2},{10,6},{14,10},{7,3},{... | collective-permute-start | bytes 3080 | tf_op jit(solution)/shard_map/ppermute | solution.py:17
Sparse Core Ops, SparseCore 0:
  8.9 83.4 all-gather.8
  94.0 79.2 all-gather.6
  174.8 79.2 all-gather.10
  255.5 79.2 all-gather.4
  340.3 26.4 reduce-scatter.2
  416.8 27.4 reduce-scatter.4
